TPU v7x, 32 devices: a whole 2x2x4 slice. The times are simulated.
32 devices in a mesh: sp: 16 (over z, x, core), tp: 2 (over y).
Axes of the slice: x: 2, y: 2, z: 4, core: 2. Of those that a mesh axis runs over, the one named last changes fastest.
Arguments:
- moe_input: bfloat16 [2048, 2048], P('sp'), may hold values from -6 to 6
- out_cotangent: bfloat16 [2048, 2048], P('sp'), may hold values from -6 to 6
- routes: int32 [2048, 2], P('sp'), may hold values from 0 to 3, all different within a row; in each aligned block of 128 rows (0 to 127, 128 to 255, ...) at most 64 rows name the same one
- route_weight: float32 [2048, 2], P('sp'), may hold values from 0.2 to 1
- w_gate: bfloat16 [16, 2048, 896], P('sp', None, 'tp'), may hold values from -0.125 to 0.125
- w_up: bfloat16 [16, 2048, 896], P('sp', None, 'tp'), may hold values from -0.125 to 0.125
- w_down: bfloat16 [16, 896, 2048], P('sp', 'tp'), may hold values from -0.09375 to 0.09375
- out_proj: bfloat16 [2048, 1024], P(None, 'tp'), may hold values from -0.243067956 to 0.243067956
- conv_out: bfloat16 [2048, 1024], P('sp', 'tp'), may hold values from -17 to 17
- glu_value: bfloat16 [2048, 1024], P('sp', 'tp'), may hold values from -6 to 6
- glu_gate: bfloat16 [2048, 1024], P('sp', 'tp'), may hold values from -9 to 9
- taps: float32 [31, 1024], P(None, 'tp'), may hold values from -1 to 1
- norm_gain: float32 [1024], P('tp'), may hold values from 0.1 to 1.9
Outputs:
- grad_gate: bfloat16 [16, 2048, 896], P('sp', None, 'tp')
- grad_up: bfloat16 [16, 2048, 896], P('sp', None, 'tp')
- grad_down: bfloat16 [16, 896, 2048], P('sp', 'tp')
- grad_proj: float32 [2048, 1024], P('sp', 'tp')
- grad_glu_value: bfloat16 [2048, 1024], P('sp', 'tp')
- grad_glu_gate: bfloat16 [2048, 1024], P('sp', 'tp')
Inputs may be any that keep to these rules, and one draw needn't show every extreme that they name: `routes`: each token names two different experts. Within the 128 tokens of one index of sp no expert is named more than 64 times, a bound that some block reaches.
All inputs are finite; a program needn't handle non-finite values.
Results may differ from a plain program's by a relative error of at most 0.014.
Values may be sent and summed in bfloat16 or wider, within the bound.
A program may use at most 128 MiB of HBM per device.

v0:
```python
import jax
import jax.numpy as jnp
from jax import lax
from jax.sharding import PartitionSpec as P

DB = 1024
WIDTH = 31
SPAN = 4


def from_partner(array, axis, distance):
    return lax.ppermute(array, axis, [(i, i ^ 1 << distance) for i in range(lax.axis_size(axis))])


def from_behind(block, axis, distance):
    devices = range(lax.axis_size(axis))
    route = [(i - distance, i) for i in devices if i - distance in devices]
    return lax.ppermute(block, axis, route)


def swish_slope(pre, sig):
    return sig * (1.0 + pre * (1.0 - sig))


def route_places(routes, experts, capacity):
    flat_routes = routes.reshape(-1)
    one_hot = (flat_routes[:, None] == jnp.arange(experts, dtype=jnp.int32)[None, :]).astype(
        jnp.int32
    )
    earlier = jnp.cumsum(one_hot, axis=0) - one_hot
    slot_index = jnp.sum(earlier * one_hot, axis=1)
    return flat_routes * capacity + slot_index


def expert_pass(expert_rows, expert_cot, w_gate, w_up, w_down):
    gate_w = w_gate[0]
    up_w = w_up[0]
    down_w = w_down[0]
    contract_rows = (((0,), (0,)), ((), ()))
    contract_units = (((1,), (1,)), ((), ()))
    gate_pre = jnp.dot(expert_rows, gate_w, preferred_element_type=jnp.float32)
    up_pre = jnp.dot(expert_rows, up_w, preferred_element_type=jnp.float32)
    gate_sig = jax.nn.sigmoid(gate_pre)
    hidden = (gate_pre * gate_sig * up_pre).astype(jnp.bfloat16)
    d_hidden = lax.dot_general(
        expert_cot, down_w, contract_units, preferred_element_type=jnp.float32
    )
    grad_down = lax.dot_general(
        hidden, expert_cot, contract_rows, preferred_element_type=jnp.float32
    ).astype(jnp.bfloat16)
    d_gate = (d_hidden * up_pre * swish_slope(gate_pre, gate_sig)).astype(jnp.bfloat16)
    d_up = (d_hidden * gate_pre * gate_sig).astype(jnp.bfloat16)
    grad_gate = lax.dot_general(
        expert_rows, d_gate, contract_rows, preferred_element_type=jnp.float32
    ).astype(jnp.bfloat16)
    grad_up = lax.dot_general(
        expert_rows, d_up, contract_rows, preferred_element_type=jnp.float32
    ).astype(jnp.bfloat16)
    total = lax.dot_general(gate_w, d_gate, contract_units, preferred_element_type=jnp.float32)
    summed = lax.psum_scatter(
        (
            total + lax.dot_general(up_w, d_up, contract_units, preferred_element_type=jnp.float32)
        ).astype(jnp.bfloat16),
        "tp",
        scatter_dimension=0,
        tiled=True,
    )
    return (grad_gate[None], grad_up[None], grad_down[None], summed)


def local(
    moe_input,
    out_cotangent,
    routes,
    route_weight,
    w_gate,
    w_up,
    w_down,
    out_proj,
    conv_out,
    glu_value,
    glu_gate,
    taps,
    norm_gain,
):
    n_sp = lax.axis_size("sp")
    experts = n_sp // SPAN
    tok_rows = routes.shape[0]
    capacity = SPAN * min(tok_rows // SPAN, 2 * tok_rows // (experts * SPAN))
    sub_cap = capacity // SPAN
    model_width = moe_input.shape[1]
    span_bits = SPAN.bit_length() - 1
    my_index = lax.axis_index("sp")
    target = route_places(routes, experts, capacity)
    matches = jnp.arange(experts * capacity, dtype=jnp.int32)[:, None] == target[None, :]
    token_ids = jnp.arange(2 * tok_rows, dtype=jnp.int32) // 2
    source = jnp.sum(jnp.where(matches, token_ids[None, :], 0), axis=1)
    weights = jnp.sum(jnp.where(matches, route_weight.reshape(-1)[None, :], 0.0), axis=1)
    filled = jnp.any(matches, axis=1)
    send_rows = jnp.where(filled[:, None], moe_input[source], jnp.zeros((), jnp.bfloat16))
    send_cot = (weights[:, None] * out_cotangent[source].astype(jnp.float32)).astype(jnp.bfloat16)
    recv_rows, recv_cot = (
        lax.all_to_all(
            send_rows.reshape(n_sp, sub_cap, model_width),
            "sp",
            split_axis=0,
            concat_axis=0,
            tiled=True,
        ),
        lax.all_to_all(
            send_cot.reshape(n_sp, sub_cap, model_width),
            "sp",
            split_axis=0,
            concat_axis=0,
            tiled=True,
        ),
    )
    stacked = jnp.stack([recv_rows, recv_cot])[:, None]
    for bit_pos in range(span_bits):
        partner = from_partner(stacked, "sp", bit_pos)
        upper = my_index >> bit_pos & 1 == 1
        stacked = jnp.where(
            upper,
            jnp.concatenate([partner, stacked], axis=1),
            jnp.concatenate([stacked, partner], axis=1),
        )
    expert_rows = stacked[0].reshape(-1, model_width)
    expert_cot = stacked[1].reshape(-1, model_width)
    grad_gate, grad_up, grad_down, row_grads = expert_pass(
        expert_rows, expert_cot, w_gate, w_up, w_down
    )
    part_width = row_grads.shape[0]
    partial_sums = row_grads.reshape(part_width, SPAN, n_sp, sub_cap)
    for section, bit_pos in enumerate(reversed(range(span_bits))):
        half = partial_sums.shape[1] // 2
        upper = my_index >> bit_pos & 1 == 1
        lower_half = partial_sums[:, :half]
        upper_half = partial_sums[:, half:]
        kept = jnp.where(upper, upper_half, lower_half)
        sent = jnp.where(upper, lower_half, upper_half)
        if section == 0:
            arrived = from_partner(sent, "sp", bit_pos)
            partial_sums = kept.astype(jnp.float32) + arrived.astype(jnp.float32)
        else:
            partial_sums = kept + from_partner(sent, "sp", bit_pos)
    returned = lax.all_to_all(partial_sums, "sp", split_axis=2, concat_axis=2, tiled=True)
    slot_grads = returned.reshape(part_width, experts * capacity)
    per_route = jnp.take(slot_grads, target, axis=1).reshape(part_width, tok_rows, 2)
    moe_grad = jnp.sum(per_route, axis=2)
    own_cot = lax.dynamic_slice_in_dim(
        out_cotangent, lax.axis_index("tp") * part_width, part_width, 1
    )
    resid_part = (own_cot.astype(jnp.float32).T + moe_grad).astype(jnp.bfloat16)
    resid_grad = lax.all_gather(resid_part, "tp", axis=0, tiled=True)
    conv_vals = conv_out.astype(jnp.float32)
    total_sum, square_sum = lax.psum(
        (jnp.sum(conv_vals, axis=1), jnp.sum(conv_vals * conv_vals, axis=1)), "tp"
    )
    mean = total_sum[:, None] / DB
    rstd = lax.rsqrt(square_sum[:, None] / DB - mean * mean + 1e-05)
    normed = (conv_vals - mean) * rstd
    zpre = normed * norm_gain[None, :]
    zsig = jax.nn.sigmoid(zpre)
    mixed = (zpre * zsig).astype(jnp.bfloat16)
    grad_proj = lax.psum_scatter(
        jnp.dot(resid_grad, mixed, preferred_element_type=jnp.float32),
        "sp",
        scatter_dimension=0,
        tiled=True,
    )
    d_mixed = lax.dot_general(
        resid_grad, out_proj, (((0,), (0,)), ((), ())), preferred_element_type=jnp.float32
    )
    d_norm = d_mixed * swish_slope(zpre, zsig) * norm_gain[None, :]
    first_sum, second_sum = lax.psum(
        (jnp.sum(d_norm, axis=1), jnp.sum(d_norm * normed, axis=1)), "tp"
    )
    conv_grad = (
        rstd * (d_norm - first_sum[:, None] / DB - normed * second_sum[:, None] / DB)
    ).astype(jnp.bfloat16)
    later_rows = from_behind(conv_grad[: WIDTH - 1], "sp", -1)
    extended = jnp.concatenate([conv_grad, later_rows], axis=0).astype(jnp.float32)
    unit_grad = lax.conv_general_dilated(
        extended[None],
        taps[:, None, :],
        (1,),
        "VALID",
        dimension_numbers=("NWC", "WIO", "NWC"),
        feature_group_count=taps.shape[1],
        precision=lax.Precision.HIGHEST,
    )[0]
    gate_sig_in = jax.nn.sigmoid(glu_gate.astype(jnp.float32))
    grad_glu_value = (unit_grad * gate_sig_in).astype(jnp.bfloat16)
    grad_glu_gate = (
        unit_grad * glu_value.astype(jnp.float32) * gate_sig_in * (1.0 - gate_sig_in)
    ).astype(jnp.bfloat16)
    return (grad_gate, grad_up, grad_down, grad_proj, grad_glu_value, grad_glu_gate)


def solution(mesh):
    in_specs = (
        P("sp", None),
        P("sp", None),
        P("sp", None),
        P("sp", None),
        P("sp", None, "tp"),
        P("sp", None, "tp"),
        P("sp", "tp", None),
        P(None, "tp"),
        P("sp", "tp"),
        P("sp", "tp"),
        P("sp", "tp"),
        P(None, "tp"),
        P("tp"),
    )
    out_specs = (
        P("sp", None, "tp"),
        P("sp", None, "tp"),
        P("sp", "tp", None),
        P("sp", "tp"),
        P("sp", "tp"),
        P("sp", "tp"),
    )
    return jax.shard_map(local, mesh=mesh, in_specs=in_specs, out_specs=out_specs, check_vma=False)
```

profile of v0, /device:TPU:15, one launch (start us, length us, event | category | flops | bytes accessed | tf_op | source)
XLA Modules:
  0.0 421.4 jit_solution(5937297597985617352)
XLA Ops:
  11.3 4.4 %gather_fusion.1 = bf16[256,2048]{1,0:T(8,128)(2,1)} fusion(bf16[128,2048]{1,0:T(8,128)(2,1)} %param.14, s32[1024]{0:T(1024)S(1)} %pad_clamp_fusion.1), kind=kCustom, calls=%fused_computation.1 | custom fusion | bytes 2098176 | tf_op jit(solution)/shard_map/gather | solution.py:101
  18.3 6.5 %all-to-all-start.1 = ((bf16[16,16,2048]{2,1,0:T(8,128)(2,1)}), bf16[16,16,2048]{2,1,0:T(8,128)(2,1)}, u32[]{:S(2)}, u32[]{:S(2)}) async-start(bf16[16,16,2048]{2,1,0:T(8,128)(2,1)} %fusion.4), calls=%async_computation.1 | async-start | bytes 2097152 | tf_op jit(solution)/shard_map/all_to_all | solution.py:110
  28.8 21.0 %all-to-all-done.1 = bf16[16,16,2048]{2,1,0:T(8,128)(2,1)} async-done(((bf16[16,16,2048]{2,1,0:T(8,128)(2,1)}), bf16[16,16,2048]{2,1,0:T(8,128)(2,1)}, u32[]{:S(2)}, u32[]{:S(2)}) %all-to-all-start.1) | async-done | bytes 1048608 | tf_op jit(solution)/shard_map/all_to_all | solution.py:110
  49.8 29.4 %all_to_all.15 = bf16[16,16,2048]{2,1,0:T(8,128)(2,1)S(1)} all-to-all(bf16[16,16,2048]{2,1,0:T(8,128)(2,1)S(1)} %broadcast_select_fusion.1), channel_id=1, replica_groups=mesh['sp'=16,'tp'=2] {'sp'}, dimensions={0} | all-to-all | bytes 2097152 | tf_op jit(solution)/shard_map/all_to_all | solution.py:103
  79.2 2.7 maximum_bitcast_fusion
  82.0 4.4 %collective-permute-done = bf16[2,1,16,16,2048]{4,3,2,0,1:T(8,128)(2,1)} collective-permute-done((bf16[2,1,16,16,2048]{4,3,2,0,1:T(8,128)(2,1)}, bf16[2,1,16,16,2048]{4,3,2,0,1:T(8,128)(2,1)}, u32[]{:S(2)}, u32[]{:S(2)}) %collective-permute-start) | collective-permute-done | bytes 2097184 | tf_op jit(solution)/shard_map/ppermute | solution.py:12
  86.4 5.8 %maximum_select_fusion.1 = bf16[2,2,16,16,2048]{4,3,2,0,1:T(8,128)(2,1)} fusion(bf16[2,1,16,16,2048]{4,3,2,0,1:T(8,128)(2,1)} %maximum_bitcast_fusion, bf16[2,1,16,16,2048]{4,3,2,0,1:T(8,128)(2,1)} %collective-permute-done, pred[]{:T(512)S(6)} %eq.45), kind=kLoop, calls=%fused_computation.6 | loop fusion | flops 6291456 | bytes 8388609 | tf_op jit(solution)/shard_map/jit(_where)/select_n | solution.py:122
  93.0 91.5 %collective-permute-done.1 = bf16[2,2,16,16,2048]{4,3,2,0,1:T(8,128)(2,1)} collective-permute-done((bf16[2,2,16,16,2048]{4,3,2,0,1:T(8,128)(2,1)}, bf16[2,2,16,16,2048]{4,3,2,0,1:T(8,128)(2,1)}, u32[]{:S(2)}, u32[]{:S(2)}) %collective-permute-start.1) | collective-permute-done | bytes 4194336 | tf_op jit(solution)/shard_map/ppermute | solution.py:12
  184.5 6.5 %maximum_select_fusion = bf16[2,4,16,16,2048]{4,3,2,0,1:T(8,128)(2,1)S(1)} fusion(bf16[2,2,16,16,2048]{4,3,2,0,1:T(8,128)(2,1)} %maximum_select_fusion.1, bf16[2,2,16,16,2048]{4,3,2,0,1:T(8,128)(2,1)} %collective-permute-done.1, pred[]{:T(512)S(6)} %eq.44), kind=kLoop, calls=%fused_computation.3 | loop fusion | flops 12582912 | bytes 16777216 | tf_op jit(solution)/shard_map/jit(_where)/select_n | solution.py:122
  203.0 4.6 %fusion = bf16[2048,1024]{0,1:T(8,128)(2,1)} fusion(f32[1024,2048]{1,0:T(8,128)S(1)} %fusion.5, bf16[1024,448]{0,1:T(8,128)(2,1)S(1)} %get-tuple-element.16, bf16[1,2048,448]{1,2,0:T(8,128)(2,1)S(1)} %copy-done.13), kind=kOutput, calls=%fused_computation.5 | convolution fusion | flops 1883242496 | bytes 15335424 | tf_op jit(solution)/shard_map/dot_general | solution.py:62
  207.6 53.8 %reduce-scatter.3.cloned.1.call-done = bf16[1024,1024]{0,1:T(8,128)(2,1)} async-done(((bf16[2048,1024]{0,1:T(8,128)(2,1)}), bf16[1024,1024]{0,1:T(8,128)(2,1)}) %reduce-scatter.3.cloned.1.call-update) | async-done | bytes 2097168 | tf_op jit(solution)/shard_map/reduce_scatter | solution.py:60
  263.6 23.6 %collective-permute-done.2 = bf16[1024,2,16,16]{0,3,1,2:T(8,128)(2,1)S(1)} collective-permute-done((bf16[1024,2,16,16]{0,3,1,2:T(8,128)(2,1)S(1)}, bf16[1024,2,16,16]{0,3,1,2:T(8,128)(2,1)S(1)}, u32[]{:S(2)}, u32[]{:S(2)}) %collective-permute-start.2) | collective-permute-done | bytes 1048608 | tf_op jit(solution)/shard_map/ppermute | solution.py:12
  293.3 6.2 %all-to-all-start.2 = ((f32[1024,1,16,16]{0,3,1,2:T(8,128)}), f32[1024,1,16,16]{0,3,1,2:T(8,128)S(1)}, u32[]{:S(2)}, u32[]{:S(2)}) async-start(f32[1024,1,16,16]{0,3,1,2:T(8,128)} %select_add_fusion), calls=%async_computation.3 | async-start | bytes 2097152 | tf_op jit(solution)/shard_map/all_to_all | solution.py:146
  300.3 3.8 all-reduce.1
  304.1 20.2 %all-to-all-done.2 = f32[1024,1,16,16]{0,3,1,2:T(8,128)S(1)} async-done(((f32[1024,1,16,16]{0,3,1,2:T(8,128)}), f32[1024,1,16,16]{0,3,1,2:T(8,128)S(1)}, u32[]{:S(2)}, u32[]{:S(2)}) %all-to-all-start.2) | async-done | bytes 1048608 | tf_op jit(solution)/shard_map/all_to_all | solution.py:146
  326.3 2.9 gather.18
  332.1 8.4 %all_gather.3 = bf16[2048,128]{0,1:T(8,128)(2,1)S(1)} all-gather(bf16[1024,128]{0,1:T(8,128)(2,1)S(1)} %fusion.16), channel_id=1, replica_groups=mesh['sp'=16,'tp'=2] {'tp'}, dimensions={0}, use_global_device_ids=true | all-gather | bytes 786432 | tf_op jit(solution)/shard_map/all_gather | solution.py:154
  340.5 2.8 fusion.43
  343.3 5.9 %fusion.2 = bf16[1,2048,448]{1,2,0:T(8,128)(2,1)} fusion(bf16[1024,448]{0,1:T(8,128)(2,1)} %copy-done.15, bf16[1024,2048]{1,0:T(8,128)(2,1)} %bitcast.98), kind=kOutput, calls=%fused_computation.11 | convolution fusion | flops 1879965696 | bytes 6946816 | tf_op jit(solution)/shard_map/dot_general | solution.py:53
  349.3 3.4 fusion.1
  353.2 3.8 all-reduce
  357.2 4.2 collective-permute-start.4
  361.4 6.0 %fusion.3 = bf16[1,2048,448]{1,2,0:T(8,128)(2,1)} fusion(bf16[1024,448]{0,1:T(8,128)(2,1)} %copy-done.16, bf16[1024,2048]{1,0:T(8,128)(2,1)} %bitcast.99), kind=kOutput, calls=%fused_computation.12 | convolution fusion | flops 1879965696 | bytes 6946816 | tf_op jit(solution)/shard_map/dot_general | solution.py:56
  369.3 45.3 %reduce-scatter.5.cloned.1.call-done = f32[128,512]{1,0:T(8,128)} async-done(((f32[2048,512]{1,0:T(8,128)}), f32[128,512]{1,0:T(8,128)}) %reduce-scatter.5.cloned.1.call-update) | async-done | bytes 262160 | tf_op jit(solution)/shard_map/reduce_scatter | solution.py:165
  (108 shorter events, 39.9 us)
Async XLA Ops:
  7.2 345.5 %copy-start = (bf16[2048,512]{1,0:T(8,128)(2,1)S(1)}, bf16[2048,512]{1,0:T(8,128)(2,1)}, u32[]{:S(2)}) copy-start(bf16[2048,512]{1,0:T(8,128)(2,1)} %param.20) | copy-start | bytes 6291460
  15.8 9.1 %copy-start.2 = (bf16[128,2048]{1,0:T(8,128)(2,1)S(1)}, bf16[128,2048]{1,0:T(8,128)(2,1)}, u32[]{:S(2)}) copy-start(bf16[128,2048]{1,0:T(8,128)(2,1)} %param.13) | copy-start | bytes 1572868
  18.3 31.5 %all-to-all-start.1 = ((bf16[16,16,2048]{2,1,0:T(8,128)(2,1)}), bf16[16,16,2048]{2,1,0:T(8,128)(2,1)}, u32[]{:S(2)}, u32[]{:S(2)}) async-start(bf16[16,16,2048]{2,1,0:T(8,128)(2,1)} %fusion.4), calls=%async_computation.1 | async-start | bytes 2097152 | tf_op jit(solution)/shard_map/all_to_all | solution.py:110
  24.8 236.6 %reduce-scatter.3.cloned.1.call-start = ((), (), s32[]{:S(2)}) async-start(), calls=%async_computation.5 | async-start | bytes 6291456 | tf_op jit(solution)/shard_map/reduce_scatter | solution.py:60
  81.9 4.5 %collective-permute-start = (bf16[2,1,16,16,2048]{4,3,2,0,1:T(8,128)(2,1)}, bf16[2,1,16,16,2048]{4,3,2,0,1:T(8,128)(2,1)}, u32[]{:S(2)}, u32[]{:S(2)}) collective-permute-start(bf16[2,1,16,16,2048]{4,3,2,0,1:T(8,128)(2,1)} %maximum_bitcast_fusion), channel_id=1, source_target_pairs={{0,2},{2,0},{4,6},{6,4},{8,10},{10,8},{12,14},{14,12},{16,18},{18,... | collective-permute-start | bytes 6291464 | tf_op jit(solution)/shard_map/ppermute | solution.py:12
  92.2 92.3 %collective-permute-start.1 = (bf16[2,2,16,16,2048]{4,3,2,0,1:T(8,128)(2,1)}, bf16[2,2,16,16,2048]{4,3,2,0,1:T(8,128)(2,1)}, u32[]{:S(2)}, u32[]{:S(2)}) collective-permute-start(bf16[2,2,16,16,2048]{4,3,2,0,1:T(8,128)(2,1)} %maximum_select_fusion.1), channel_id=1, source_target_pairs={{0,4},{2,6},{4,0},{6,2},{8,12},{10,14},{12,8},{14,10},{16,20},{18,... | collective-permute-start | bytes 12582920 | tf_op jit(solution)/shard_map/ppermute | solution.py:12
  192.4 5.1 %copy-start.4 = (bf16[1,4,16,16,2048]{4,3,2,0,1:T(8,128)(2,1)}, bf16[1,4,16,16,2048]{4,3,2,0,1:T(8,128)(2,1)S(1)}, u32[]{:S(2)}) copy-start(bf16[1,4,16,16,2048]{4,3,2,0,1:T(8,128)(2,1)S(1)} %get-tuple-element.14) | copy-start | bytes 12582916
  192.5 2.9 copy-start.13
  195.4 2.5 copy-start.11
  197.5 3.1 copy-start.19
  200.6 2.4 copy-start.15
  263.3 23.9 %collective-permute-start.2 = (bf16[1024,2,16,16]{0,3,1,2:T(8,128)(2,1)S(1)}, bf16[1024,2,16,16]{0,3,1,2:T(8,128)(2,1)S(1)}, u32[]{:S(2)}, u32[]{:S(2)}) collective-permute-start(bf16[1024,2,16,16]{0,3,1,2:T(8,128)(2,1)S(1)} %broadcast_select_fusion), channel_id=1, source_target_pairs={{0,4},{2,6},{4,0},{6,2},{8,12},{10,14},{12,8},{14,10},{16,20},{18,... | collective-permute-start | bytes 3145736 | tf_op jit(solution)/shard_map/ppermute | solution.py:12
  288.0 4.0 collective-permute-start.3
  293.3 6.4 %copy-start.9 = (s32[128,2]{0,1:T(2,128)S(1)}, s32[128,2]{0,1:T(2,128)}, u32[]{:S(2)}) copy-start(s32[128,2]{0,1:T(2,128)} %param.15) | copy-start | bytes 3076
  293.3 6.9 %copy-start.6 = (bf16[128,512]{1,0:T(8,128)(2,1)S(1)}, bf16[128,512]{1,0:T(8,128)(2,1)}, u32[]{:S(2)}) copy-start(bf16[128,512]{1,0:T(8,128)(2,1)} %param.21) | copy-start | bytes 393220
  293.3 31.0 %all-to-all-start.2 = ((f32[1024,1,16,16]{0,3,1,2:T(8,128)}), f32[1024,1,16,16]{0,3,1,2:T(8,128)S(1)}, u32[]{:S(2)}, u32[]{:S(2)}) async-start(f32[1024,1,16,16]{0,3,1,2:T(8,128)} %select_add_fusion), calls=%async_computation.3 | async-start | bytes 2097152 | tf_op jit(solution)/shard_map/all_to_all | solution.py:146
  299.5 115.1 %reduce-scatter.5.cloned.1.call-start = ((), (), s32[]{:S(2)}) async-start(), calls=%async_computation.6 | async-start | bytes 4456448 | tf_op jit(solution)/shard_map/reduce_scatter | solution.py:165
  326.3 5.7 %copy-start.1 = (bf16[128,2048]{1,0:T(8,128)(2,1)S(1)}, bf16[128,2048]{1,0:T(8,128)(2,1)}, u32[]{:S(2)}) copy-start(bf16[128,2048]{1,0:T(8,128)(2,1)} %param.14) | copy-start | bytes 1572868
  329.3 11.2 %copy-start.10 = (f32[512]{0:T(512)S(1)}, f32[512]{0:T(512)}, u32[]{:S(2)}) copy-start(f32[512]{0:T(512)} %param.25) | copy-start | bytes 6148
  343.3 5.9 %copy-start.5 = (bf16[1,4,16,16,2048]{4,3,2,0,1:T(8,128)(2,1)S(1)}, bf16[1,4,16,16,2048]{4,3,2,0,1:T(8,128)(2,1)}, u32[]{:S(2)}) copy-start(bf16[1,4,16,16,2048]{4,3,2,0,1:T(8,128)(2,1)} %copy-done.4) | copy-start | bytes 12582916
  343.3 5.9 %copy-start.18 = (f32[1024,448]{0,1:T(8,128)S(1)}, f32[1024,448]{0,1:T(8,128)}, u32[]{:S(2)}) copy-start(f32[1024,448]{0,1:T(8,128)} %copy-done.17) | copy-start | bytes 5505028
  343.3 5.9 %copy-start.20 = (f32[1024,448]{0,1:T(8,128)S(1)}, f32[1024,448]{0,1:T(8,128)}, u32[]{:S(2)}) copy-start(f32[1024,448]{0,1:T(8,128)} %copy-done.19) | copy-start | bytes 5505028
  357.2 10.2 %copy-start.14 = (f32[31,512]{1,0:T(8,128)S(1)}, f32[31,512]{1,0:T(8,128)}, u32[]{:S(2)}) copy-start(f32[31,512]{1,0:T(8,128)} %param.24) | copy-start | bytes 190468
  357.2 10.2 %collective-permute-start.4 = (bf16[30,512]{1,0:T(8,128)(2,1)S(1)}, bf16[30,512]{1,0:T(8,128)(2,1)S(1)}, u32[]{:S(2)}, u32[]{:S(2)}) collective-permute-start(bf16[30,512]{1,0:T(8,128)(2,1)S(1)} %slice.49), channel_id=1, source_target_pairs={{2,0},{4,2},{6,4},{8,6},{10,8},{12,10},{14,12},{16,14},{18,16},{20... | collective-permute-start | bytes 92168 | tf_op jit(solution)/shard_map/ppermute | solution.py:18
  (6 other events, 10.4 us)
Sparse Core Ops, SparseCore 0:
  207.7 53.6 reduce-scatter.2
  343.4 71.1 reduce-scatter.4
where the time goes:
time: 426 us; the launch traced here: 421 us
  waiting for transfers between devices  262 us (62%)
  blocking collectives  45.4 us (11%)
  matrix products  33.6 us (8%)
  other arithmetic  26.6 us (6%)
  starting transfers between devices  20 us (5%)
  local copies, waits for them, and re-layouts  19.3 us (5%)
  between operations  14.5 us (3%)
    ppermute x4, waiting for transfers between devices, from_partner(): lax.ppermute(array, axis, [(i, i ^ 1 << distance) for i in range(lax.axis...  122 us
    reduce_scatter x1, waiting for transfers between devices, expert_pass(): lax.psum_scatter((total + lax.dot_general(up_w, d_up, contract_units, pre...  53.8 us
    reduce_scatter x1, waiting for transfers between devices, local(): lax.psum_scatter(jnp.dot(resid_grad, mixed, preferred_element_type=jnp.fl...  45.3 us
    all_to_all x1, blocking collectives, local(): lax.all_to_all(send_rows.reshape(n_sp, sub_cap, model_width), 'sp', split...  29.4 us
    all_to_all x1, waiting for transfers between devices, local(): lax.all_to_all(send_cot.reshape(n_sp, sub_cap, model_width), 'sp', split_...  21 us
    all_to_all x1, waiting for transfers between devices, local(): lax.all_to_all(partial_sums, 'sp', split_axis=2, concat_axis=2, tiled=True)  20.2 us
    select_n x2, other arithmetic, local(): jnp.where(upper, jnp.concatenate([partner, stacked], axis=1), jnp.concate...  12.3 us
  transfers between devices with their start and end apart: 9, of which 8 were waited for; matrix products, arithmetic and copies ran while one was open for 5% of the time, Pallas kernels for 0%

commit v1 on v0

--- a/solution.py
+++ b/solution.py
@@ -1,7 +1,16 @@
+import functools
+
 import jax
 import jax.numpy as jnp
 from jax import lax
+from jax.experimental import pallas as pl
+from jax.experimental.pallas import tpu as pltpu
 from jax.sharding import PartitionSpec as P
+
+F32 = jnp.float32
+BF16 = jnp.bfloat16
+ROWS = (((0,), (0,)), ((), ()))
+UNITS = (((1,), (1,)), ((), ()))
 
 DB = 1024
 WIDTH = 31
@@ -197,6 +206,497 @@
     return (grad_gate, grad_up, grad_down, grad_proj, grad_glu_value, grad_glu_gate)
 
 
+def send(src, dst, send_sem, recv_sem, sp, tp):
+    return pltpu.make_async_remote_copy(
+        src_ref=src,
+        dst_ref=dst,
+        send_sem=send_sem,
+        recv_sem=recv_sem,
+        device_id={"sp": sp, "tp": tp},
+        device_id_type=pl.DeviceIdType.MESH,
+    )
+
+
+def greet(peers):
+    barrier = pltpu.get_barrier_semaphore()
+    for sp, tp in peers:
+        pl.semaphore_signal(
+            barrier, inc=1, device_id={"sp": sp, "tp": tp}, device_id_type=pl.DeviceIdType.MESH
+        )
+    return lambda: pl.semaphore_wait(barrier, len(peers))
+
+
+def near_first(groups):
+    order = [0]
+    for step in range(1, groups // 2 + 1):
+        order += [step] if step == groups - step else [step, groups - step]
+    return order if groups > 1 else [0]
+
+
+def place():
+    s, t = lax.axis_index("sp"), lax.axis_index("tp")
+    q, r = s // SPAN, s % SPAN
+    x, c = r // 2, r % 2
+    rx = 2 * (1 - x) + c
+    rc = 2 * x + 1 - c
+    rxc = 2 * (1 - x) + 1 - c
+    return s, t, 1 - t, q, r, x, c, rx, rc, rxc
+
+
+def dispatch_kernel(
+    groups, x_ref, g_ref, routes_ref, weight_ref, conv_ref, gain_ref,
+    xo, mo, pt_ref, stat_ref,
+    sb, xs, ms, st, st_in,
+    z_s, z_r, x_s, x_r, y_s, y_r, a_s, a_r, b_s, b_r, c_s, c_r,
+    mz_s, mz_r, mx_s, mx_r, mc_s, mc_r, st_s, st_r, o_s, mo_s,
+):
+    s, t, u, q, r, _, _, rx, rc, rxc = place()
+    n_sp = groups * SPAN
+    tok, width = x_ref.shape
+    cap = sb.shape[2]
+    half = width // 2
+    mine = pl.ds(pl.multiple_of(t * half, 128), half)
+    other = pl.ds(pl.multiple_of(u * half, 128), half)
+    order = near_first(groups)
+    at_x, at_c, at_y = (q * SPAN + rx, t), (q * SPAN + rc, t), (s, u)
+    peers = [(lax.rem(q + d, groups) * SPAN + r, t) for d in order[1:]]
+    ready = greet(peers + [at_x, at_c, at_y])
+
+    lane = lax.broadcasted_iota(jnp.int32, (tok, 128), 1)
+    hot = [(routes_ref[:, k : k + 1] == lane).astype(F32) for k in range(2)]
+    before = (
+        lax.broadcasted_iota(jnp.int32, (tok, tok), 1) < lax.broadcasted_iota(jnp.int32, (tok, tok), 0)
+    ).astype(BF16)
+    counts = jnp.dot(before, (hot[0] + hot[1]).astype(BF16), preferred_element_type=F32)
+    spots = lax.broadcasted_iota(jnp.int32, (tok, groups * cap), 1)
+    pts, cots = [], []
+    for k in range(2):
+        slot = jnp.sum(counts * hot[k], axis=1, keepdims=True).astype(jnp.int32)
+        target = routes_ref[:, k : k + 1] * cap + slot
+        pts.append((target == spots).astype(F32).astype(BF16))
+    pt = pts[0] + pts[1]
+    pt_ref[...] = pt
+    chunk = 512
+    for j in range(0, width, chunk):
+        cols = slice(j, j + chunk)
+        rows = lax.dot_general(pt, x_ref[:, cols], ROWS, preferred_element_type=F32)
+        sb[0, :, :, cols] = rows.astype(BF16).reshape(groups, cap, chunk)
+        cot = g_ref[:, cols].astype(F32)
+        total = None
+        for k in range(2):
+            part = lax.dot_general(
+                pts[k],
+                (weight_ref[:, k : k + 1] * cot).astype(BF16),
+                ROWS,
+                preferred_element_type=F32,
+            )
+            total = part if total is None else total + part
+        sb[1, :, :, cols] = total.astype(BF16).reshape(groups, cap, chunk)
+    conv = conv_ref[...].astype(F32)
+    first = jnp.sum(conv, axis=1, keepdims=True)
+    second = jnp.sum(conv * conv, axis=1, keepdims=True)
+    st[...] = jnp.where(lane == 0, first, second)
+    ready()
+
+    started = []
+
+    def go(copy):
+        copy.start()
+        started.append(copy)
+
+    for d in order[1:]:
+        to = lax.rem(q + d, groups)
+        go(send(sb.at[:, to, :, mine], xs.at[:, s, :, mine], z_s.at[d], z_r.at[d], to * SPAN + r, t))
+    go(send(st, st_in, st_s, st_r, *at_y))
+
+    def stage_one(d):
+        b = lax.rem(q - d + groups, groups) * SPAN + r
+        dst = xs.at[:, b, :, mine]
+        if d:
+            send(dst, dst, z_s.at[d], z_r.at[d], s, t).wait_recv()
+        src = dst if d else sb.at[:, q, :, mine]
+        go(send(src, dst, x_s.at[d], x_r.at[d], *at_x))
+        go(send(src, dst, y_s.at[d], y_r.at[d], *at_y))
+        go(send(src, dst, c_s.at[d, 0], c_r.at[d, 0], *at_c))
+
+    def diag_a(d):
+        return pl.ds(0, 2) if d == 0 else pl.ds(0, 1)
+
+    def stage_two(d):
+        base = lax.rem(q - d + groups, groups) * SPAN
+        got = xs.at[:, base + rx, :, mine]
+        send(got, got, x_s.at[d], x_r.at[d], *at_x).wait_recv()
+        part = xs.at[diag_a(d), base + rx, :, mine]
+        go(send(part, part, a_s.at[d], a_r.at[d], *at_y))
+        go(send(got, got, c_s.at[d, 1], c_r.at[d, 1], *at_c))
+        got = xs.at[:, base + r, :, other]
+        send(got, got, y_s.at[d], y_r.at[d], *at_y).wait_recv()
+        if d:
+            part = xs.at[pl.ds(1, 1), base + r, :, other]
+            go(send(part, part, b_s.at[d], b_r.at[d], *at_x))
+        go(send(got, got, c_s.at[d, 2], c_r.at[d, 2], *at_c))
+
+    def stage_three(d):
+        b = lax.rem(q - d + groups, groups) * SPAN + rx
+        part = xs.at[diag_a(d), b, :, other]
+        send(part, part, a_s.at[d], a_r.at[d], *at_y).wait_recv()
+        if d:
+            part = xs.at[pl.ds(1, 1), b, :, other]
+            send(part, part, b_s.at[d], b_r.at[d], *at_x).wait_recv()
+        got = xs.at[:, b, :, other]
+        go(send(got, got, c_s.at[d, 3], c_r.at[d, 3], *at_c))
+
+    def finish(d):
+        base = lax.rem(q - d + groups, groups) * SPAN
+        for i, (place_in, cols) in enumerate([(rc, mine), (rxc, mine), (rc, other), (rxc, other)]):
+            got = xs.at[:, base + place_in, :, cols]
+            send(got, got, c_s.at[d, i], c_r.at[d, i], *at_c).wait_recv()
+        span = pl.ds(base, SPAN)
+        out = pltpu.make_async_copy(xs.at[:, span], xo.at[:, span], o_s.at[d])
+        out.start()
+        return out
+
+    stage_one(0)
+    xs[:, s, :, mine] = sb[:, q, :, mine]
+    send(st, st_in, st_s, st_r, *at_y).wait_recv()
+    sums = st[...] + st_in[...]
+    channels = conv_ref.shape[1] * 2
+    mean = sums[:, 0:1] / channels
+    rstd = lax.rsqrt(sums[:, 1:2] / channels - mean * mean + 1e-05)
+    stat_ref[...] = jnp.where(lane == 0, mean, rstd)
+    zpre = (conv - mean) * rstd * gain_ref[...]
+    ms[s] = (zpre * jax.nn.sigmoid(zpre)).astype(BF16)
+    for d in order[1:]:
+        to = lax.rem(q + d, groups)
+        go(send(ms.at[s], ms.at[s], mz_s.at[d], mz_r.at[d], to * SPAN + r, t))
+
+    outs = []
+    for i in range(groups + 2):
+        if 0 < i < groups:
+            stage_one(order[i])
+        if 0 < i <= groups:
+            stage_two(order[i - 1])
+        if i > 1:
+            stage_three(order[i - 2])
+            d = order[i - 2]
+            got = ms.at[lax.rem(q - d + groups, groups) * SPAN + r]
+            if d:
+                send(got, got, mz_s.at[d], mz_r.at[d], s, t).wait_recv()
+            go(send(got, got, mx_s.at[d], mx_r.at[d], *at_x))
+            go(send(got, got, mc_s.at[d, 0], mc_r.at[d, 0], *at_c))
+    for d in order:
+        outs.append(finish(d))
+    for d in order:
+        got = ms.at[lax.rem(q - d + groups, groups) * SPAN + rx]
+        send(got, got, mx_s.at[d], mx_r.at[d], *at_x).wait_recv()
+        go(send(got, got, mc_s.at[d, 1], mc_r.at[d, 1], *at_c))
+    for d in order:
+        base = lax.rem(q - d + groups, groups) * SPAN
+        for i, place_in in enumerate([rc, rxc]):
+            got = ms.at[base + place_in]
+            send(got, got, mc_s.at[d, i], mc_r.at[d, i], *at_c).wait_recv()
+    out = pltpu.make_async_copy(ms, mo, mo_s)
+    out.start()
+    outs.append(out)
+    for copy in started:
+        copy.wait_send()
+    for copy in outs:
+        copy.wait()
+
+
+def combine_kernel(
+    groups, t_ref, pt_ref, stat_ref, g_ref, proj_ref, conv_ref, gain_ref, value_ref, gate_ref, taps_ref, m_ref,
+    gp_ref, gv_ref, gg_ref,
+    core_in, s1, rx1, ry1, sa, sbb, rx2, ry2, fin, rz, rt, rr, st, st_in, ext, halo, halo_in, slope_ref, normed_ref,
+    c_s, c_r, x1_s, x1_r, y1_s, y1_r, x2_s, x2_r, y2_s, y2_r, z_s, z_r,
+    h_s, h_r, k_s, k_r, st_s, st_r, halo_s, halo_r,
+):
+    s, t, u, q, r, x, c, rx, rc, _ = place()
+    xb, cb = 1 - x, 1 - c
+    n_sp = groups * SPAN
+    tok, width = g_ref.shape
+    cap = t_ref.shape[1]
+    half = width // 2
+    piece = half // 2
+    block = width // n_sp
+    order = near_first(groups)[::-1]
+    at_x, at_c, at_y = (q * SPAN + rx, t), (q * SPAN + rc, t), (s, u)
+    ready = greet([(lax.rem(s + d, n_sp), t) for d in range(1, n_sp)] + [at_y])
+    lane = lax.broadcasted_iota(jnp.int32, (tok, 128), 1)
+    started = []
+
+    def go(copy):
+        copy.start()
+        started.append(copy)
+
+    def recv(dst, recv_sem):
+        send(dst, dst, recv_sem, recv_sem, *at_y).wait_recv()
+
+    def add(a, b):
+        return (a.astype(F32) + b.astype(F32)).astype(BF16)
+
+    ready()
+    for d in order:
+        to = lax.rem(q + d, groups)
+        for i in range(2):
+            go(send(t_ref.at[to * SPAN + 2 * i + cb], core_in.at[d, i], c_s.at[d, i], c_r.at[d, i], *at_c))
+
+    def stage_one(d):
+        to = lax.rem(q + d, groups)
+        for i in range(2):
+            recv(core_in.at[d, i], c_r.at[d, i])
+            for h in range(2):
+                for p in range(2):
+                    cols = slice(h * half + p * piece, h * half + (p + 1) * piece)
+                    s1[d, i, p, h] = add(t_ref[to * SPAN + 2 * i + c, :, cols], core_in[d, i, :, cols])
+        go(send(s1.at[d, xb, 0], rx1.at[d], x1_s.at[d], x1_r.at[d], *at_x))
+        go(send(s1.at[d, :, 1, u], ry1.at[d], y1_s.at[d], y1_r.at[d], *at_y))
+
+    def stage_two(d):
+        recv(rx1.at[d], x1_r.at[d])
+        for h in range(2):
+            sa[d, h] = add(s1[d, x, 0, h], rx1[d, h])
+        go(send(sa.at[d, u], ry2.at[d], y2_s.at[d], y2_r.at[d], *at_y))
+        recv(ry1.at[d], y1_r.at[d])
+        for i in range(2):
+            sbb[d, i] = add(s1[d, i, 1, t], ry1[d, i])
+        go(send(sbb.at[d, xb], rx2.at[d], x2_s.at[d], x2_r.at[d], *at_x))
+
+    def stage_three(d):
+        recv(ry2.at[d], y2_r.at[d])
+        low = add(sa[d, t], ry2[d])
+        recv(rx2.at[d], x2_r.at[d])
+        high = add(sbb[d, x], rx2[d])
+        if d:
+            fin[d, :, :piece] = low
+            fin[d, :, piece:] = high
+            to = lax.rem(q + d, groups) * SPAN + r
+            go(send(fin.at[d], rz.at[q], z_s.at[d], z_r.at[d], to, t))
+        else:
+            rz[q, :, :piece] = low
+            rz[q, :, piece:] = high
+
+    for i in range(groups + 2):
+        if i < groups:
+            stage_one(order[i])
+        if i == 1:
+            normed = (conv_ref[...].astype(F32) - stat_ref[:, 0:1]) * stat_ref[:, 1:2]
+            zpre = normed * gain_ref[...]
+            sig = jax.nn.sigmoid(zpre)
+            normed_ref[...] = normed
+            slope_ref[...] = swish_slope(zpre, sig) * gain_ref[...]
+        if 0 < i <= groups:
+            stage_two(order[i - 1])
+        if i > 1:
+            stage_three(order[i - 2])
+    for d in order:
+        if d:
+            recv(rz.at[lax.rem(q - d + groups, groups)], z_r.at[d])
+
+    eye = (
+        lax.broadcasted_iota(jnp.int32, (tok, tok), 0) == lax.broadcasted_iota(jnp.int32, (tok, tok), 1)
+    ).astype(F32).astype(BF16)
+    pt = pt_ref[...]
+    chunk = 256
+    for j in range(0, half, chunk):
+        own = g_ref[:, pl.ds(pl.multiple_of(t * half + j, 128), chunk)]
+        slots = rz[:, :, j : j + chunk].reshape(groups * cap, chunk)
+        total = lax.dot_general(own, eye, ROWS, preferred_element_type=F32) + lax.dot_general(
+            slots, pt, (((0,), (1,)), ((), ())), preferred_element_type=F32
+        )
+        rt[pl.ds(pl.multiple_of(t * half + j, 128), chunk), :] = total.astype(BF16)
+    mine = rt.at[pl.ds(pl.multiple_of(t * half, 128), half)]
+    other = rt.at[pl.ds(pl.multiple_of(u * half, 128), half)]
+    go(send(mine, mine, h_s, h_r, *at_y))
+
+    def rows_of(to):
+        return rt.at[pl.ds(pl.multiple_of(to * block, block), block)]
+
+    def column_of(source):
+        return rr.at[:, pl.ds(pl.multiple_of(source * tok, 128), tok)]
+
+    def scatter(part):
+        for d in range(n_sp // 2):
+            to = part * (n_sp // 2) + lax.rem(s + d, n_sp // 2)
+
+            @pl.when(to != s)
+            def _():
+                send(rows_of(to), column_of(s), k_s.at[to], k_r.at[s], to, t).start()
+
+    scatter(t)
+    recv(other, h_r)
+    scatter(u)
+    rr[:, pl.ds(pl.multiple_of(s * tok, 128), tok)] = rt[pl.ds(pl.multiple_of(s * block, block), block), :]
+
+    d_mixed = lax.dot_general(rt[...], proj_ref[...], ROWS, preferred_element_type=F32)
+    channels = 2 * conv_ref.shape[1]
+    d_norm = d_mixed * slope_ref[...]
+    normed = normed_ref[...]
+    first = jnp.sum(d_norm, axis=1, keepdims=True)
+    second = jnp.sum(d_norm * normed, axis=1, keepdims=True)
+    st[...] = jnp.where(lane == 0, first, second)
+    go(send(st, st_in, st_s, st_r, *at_y))
+    recv(st_in, st_r)
+    sums = st[...] + st_in[...]
+    conv_grad = stat_ref[:, 1:2] * (
+        d_norm - sums[:, 0:1] / channels - normed * (sums[:, 1:2] / channels)
+    )
+    conv_grad = conv_grad.astype(BF16)
+    reach = halo.shape[0]
+    halo[...] = conv_grad[:reach]
+
+    @pl.when(s > 0)
+    def _():
+        send(halo, halo_in, halo_s, halo_r, s - 1, t).start()
+
+    ext[:tok] = conv_grad.astype(F32)
+    halo_in_needed = s < n_sp - 1
+
+    @pl.when(halo_in_needed)
+    def _():
+        recv(halo_in, halo_r)
+        ext[tok:] = halo_in[...].astype(F32)
+
+    @pl.when(jnp.logical_not(halo_in_needed))
+    def _():
+        ext[tok:] = jnp.zeros((reach, ext.shape[1]), F32)
+
+    lanes = 128
+    for j in range(0, ext.shape[1], lanes):
+        cols = slice(j, j + lanes)
+        total = taps_ref[0:1, cols] * ext[0:tok, cols]
+        for k in range(1, taps_ref.shape[0]):
+            total = total + taps_ref[k : k + 1, cols] * ext[k : k + tok, cols]
+        sig = jax.nn.sigmoid(gate_ref[:, cols].astype(F32))
+        gv_ref[:, cols] = (total * sig).astype(BF16)
+        gg_ref[:, cols] = (total * value_ref[:, cols].astype(F32) * sig * (1.0 - sig)).astype(BF16)
+
+    for d in range(1, n_sp):
+        source = lax.rem(s + n_sp - d, n_sp)
+        recv(column_of(source), k_r.at[source])
+    gp_ref[...] = jnp.dot(
+        rr[...], m_ref[...].reshape(n_sp * tok, m_ref.shape[2]), preferred_element_type=F32
+    )
+    for copy in started:
+        copy.wait_send()
+
+    @pl.when(s > 0)
+    def _():
+        send(halo, halo_in, halo_s, halo_r, s - 1, t).wait_send()
+
+    for d in range(1, n_sp):
+        to = lax.rem(s + d, n_sp)
+        send(rows_of(to), column_of(s), k_s.at[to], k_r.at[s], to, t).wait_send()
+
+
+def paired(
+    moe_input, out_cotangent, routes, route_weight, w_gate, w_up, w_down, out_proj, conv_out, glu_value, glu_gate, taps, norm_gain
+):
+    n_sp = lax.axis_size("sp")
+    groups = n_sp // SPAN
+    tok, width = moe_input.shape
+    channels = conv_out.shape[1]
+    cap = SPAN * min(tok // SPAN, 2 * tok // (groups * SPAN))
+    vmem = pl.BlockSpec(memory_space=pltpu.VMEM)
+    hbm = pl.BlockSpec(memory_space=pl.ANY)
+    dma = pltpu.SemaphoreType.DMA
+    gain = norm_gain[None]
+    rows, mixed_all, pt, stat = pl.pallas_call(
+        functools.partial(dispatch_kernel, groups),
+        out_shape=(
+            jax.ShapeDtypeStruct((2, n_sp, cap, width), BF16),
+            jax.ShapeDtypeStruct((n_sp, tok, channels), BF16),
+            jax.ShapeDtypeStruct((tok, groups * cap), BF16),
+            jax.ShapeDtypeStruct((tok, 128), F32),
+        ),
+        in_specs=[vmem] * 6,
+        out_specs=(hbm, hbm, vmem, vmem),
+        scratch_shapes=[
+            pltpu.VMEM((2, groups, cap, width), BF16),
+            pltpu.VMEM((2, n_sp, cap, width), BF16),
+            pltpu.VMEM((n_sp, tok, channels), BF16),
+            pltpu.VMEM((tok, 128), F32),
+            pltpu.VMEM((tok, 128), F32),
+        ]
+        + [dma((groups,))] * 10
+        + [dma((groups, 4))] * 2
+        + [dma((groups,))] * 4
+        + [dma((groups, 2))] * 2
+        + [dma] * 2
+        + [dma((groups,)), dma],
+        compiler_params=pltpu.CompilerParams(
+            collective_id=0, has_side_effects=True, vmem_limit_bytes=36 << 20
+        ),
+        name="dispatch",
+    )(moe_input, out_cotangent, routes, route_weight, conv_out, gain)
+    expert_rows = rows[0].reshape(n_sp * cap, width)
+    expert_cot = rows[1].reshape(n_sp * cap, width)
+    grad_gate, grad_up, grad_down, part = expert_products(expert_rows, expert_cot, w_gate, w_up, w_down)
+    reach = -(-(WIDTH - 1) // 16) * 16
+    half = width // 2
+    piece = half // 2
+    pair = pltpu.VMEM((groups, 2, cap, piece), BF16)
+    single = pltpu.VMEM((groups, cap, piece), BF16)
+    grad_proj, grad_value, grad_gate_in = pl.pallas_call(
+        functools.partial(combine_kernel, groups),
+        out_shape=(
+            jax.ShapeDtypeStruct((width // n_sp, channels), F32),
+            jax.ShapeDtypeStruct((tok, channels), BF16),
+            jax.ShapeDtypeStruct((tok, channels), BF16),
+        ),
+        in_specs=[vmem] * 11,
+        out_specs=(vmem,) * 3,
+        scratch_shapes=[
+            pltpu.VMEM((groups, 2, cap, width), BF16),
+            pltpu.VMEM((groups, 2, 2, 2, cap, piece), BF16),
+            pair, pair, pair, pair, single, single,
+            pltpu.VMEM((groups, cap, half), BF16),
+            pltpu.VMEM((groups, cap, half), BF16),
+            pltpu.VMEM((width, tok), BF16),
+            pltpu.VMEM((width // n_sp, n_sp * tok), BF16),
+            pltpu.VMEM((tok, 128), F32),
+            pltpu.VMEM((tok, 128), F32),
+            pltpu.VMEM((tok + reach, channels), F32),
+            pltpu.VMEM((reach, channels), BF16),
+            pltpu.VMEM((reach, channels), BF16),
+            pltpu.VMEM((tok, channels), F32),
+            pltpu.VMEM((tok, channels), F32),
+        ]
+        + [dma((groups, 2))] * 2
+        + [dma((groups,))] * 10
+        + [dma] * 2
+        + [dma((n_sp,))] * 2
+        + [dma] * 4,
+        compiler_params=pltpu.CompilerParams(
+            collective_id=1, has_side_effects=True, vmem_limit_bytes=48 << 20
+        ),
+        name="combine",
+    )(
+        part.reshape(n_sp, cap, width),
+        pt, stat, out_cotangent, out_proj, conv_out, gain, glu_value, glu_gate, taps, mixed_all,
+    )
+    return (grad_gate, grad_up, grad_down, grad_proj, grad_value, grad_gate_in)
+
+
+def expert_products(expert_rows, expert_cot, w_gate, w_up, w_down):
+    gate_w, up_w, down_w = w_gate[0], w_up[0], w_down[0]
+    gate_pre = jnp.dot(expert_rows, gate_w, preferred_element_type=F32)
+    up_pre = jnp.dot(expert_rows, up_w, preferred_element_type=F32)
+    gate_sig = jax.nn.sigmoid(gate_pre)
+    hidden = (gate_pre * gate_sig * up_pre).astype(BF16)
+    d_hidden = lax.dot_general(expert_cot, down_w, UNITS, preferred_element_type=F32)
+    grad_down = lax.dot_general(hidden, expert_cot, ROWS, preferred_element_type=F32).astype(BF16)
+    d_gate = (d_hidden * up_pre * swish_slope(gate_pre, gate_sig)).astype(BF16)
+    d_up = (d_hidden * gate_pre * gate_sig).astype(BF16)
+    grad_gate = lax.dot_general(expert_rows, d_gate, ROWS, preferred_element_type=F32).astype(BF16)
+    grad_up = lax.dot_general(expert_rows, d_up, ROWS, preferred_element_type=F32).astype(BF16)
+    part = (
+        lax.dot_general(d_gate, gate_w, UNITS, preferred_element_type=F32)
+        + lax.dot_general(d_up, up_w, UNITS, preferred_element_type=F32)
+    ).astype(BF16)
+    return grad_gate[None], grad_up[None], grad_down[None], part
+
+
 def solution(mesh):
     in_specs = (
         P("sp", None),
@@ -221,4 +721,5 @@
         P("sp", "tp"),
         P("sp", "tp"),
     )
-    return jax.shard_map(local, mesh=mesh, in_specs=in_specs, out_specs=out_specs, check_vma=False)
+    body = paired if mesh.shape["tp"] == 2 else local
+    return jax.shard_map(body, mesh=mesh, in_specs=in_specs, out_specs=out_specs, check_vma=False)

time: 426 us -> 140 us (0.33); the launches traced: 421 us -> 140 us
  waiting for transfers between devices: 262 us -> 0 us
  Pallas kernels: 0 us -> 106 us
  blocking collectives: 45.4 us -> 0 us
  other arithmetic: 26.6 us -> 0 us
  starting transfers between devices: 20 us -> 0 us
  between operations: 14.5 us -> 0.81 us
  local copies, waits for them, and re-layouts: 19.3 us -> 8.53 us
  matrix products: 33.6 us -> 24.1 us
    ppermute x5 -> x0, waiting for transfers between devices: 122 us -> none  [the longest x4 122 us: from_partner(): lax.ppermute(array, axis, [(i, i ^ 1 << distance) for i in range(lax.axis...]
    pallas_call x0 -> x2, Pallas kernels: none -> 106 us  [the longest x1 55.1 us: paired(): pl.pallas_call(functools.partial(combine_kernel, groups), out_shape=(jax....]
    reduce_scatter x2 -> x0, waiting for transfers between devices: 99.1 us -> none  [the longest x1 53.8 us: expert_pass(): lax.psum_scatter((total + lax.dot_general(up_w, d_up, contract_units, pre...]
    all_to_all x2 -> x0, waiting for transfers between devices: 41.2 us -> none  [the longest x1 21 us: local(): lax.all_to_all(send_cot.reshape(n_sp, sub_cap, model_width), 'sp', split_...]
    all_to_all x1 -> x0, blocking collectives: 29.4 us -> none  [local(): lax.all_to_all(send_rows.reshape(n_sp, sub_cap, model_width), 'sp', split...]
    select_n x8 -> x0, other arithmetic: 13.9 us -> none  [the longest x2 12.3 us: local(): jnp.where(upper, jnp.concatenate([partner, stacked], axis=1), jnp.concate...]
    all_to_all x2 -> x0, starting transfers between devices: 12.7 us -> none  [the longest x1 6.52 us: local(): lax.all_to_all(send_cot.reshape(n_sp, sub_cap, model_width), 'sp', split_...]
    gather x4 -> x0, local copies, waits for them, and re-layouts: 11.7 us -> none  [the longest x2 4.96 us: local(): jnp.take(slot_grads, target, axis=1).reshape(part_width, tok_rows, 2)]
  transfers between devices with their start and end apart: 9 -> 0, of which waited for: 8 -> 0; matrix products, arithmetic and copies ran while one was open for 5% -> 0% of each run, Pallas kernels for 0% -> 0%
where the time goes in v1:
time: 140 us
  Pallas kernels  106 us (76%)
  matrix products  24.1 us (17%)
  local copies, waits for them, and re-layouts  8.53 us (6%)
    pallas_call x1, Pallas kernels, paired(): pl.pallas_call(functools.partial(combine_kernel, groups), out_shape=(jax....  55.1 us
    pallas_call x1, Pallas kernels, paired(): pl.pallas_call(functools.partial(dispatch_kernel, groups), out_shape=(jax...  51.2 us
    unnamed x33, local copies, waits for them, and re-layouts  7.45 us
    dot_general x1, matrix products, expert_products(): lax.dot_general(d_up, up_w, UNITS, preferred_element_type=F32)  4.56 us
    dot_general x1, matrix products, expert_products(): lax.dot_general(hidden, expert_cot, ROWS, preferred_element_type=F32)  3.37 us
    dot_general x1, matrix products, expert_products(): lax.dot_general(expert_rows, d_up, ROWS, preferred_element_type=F32)  3.33 us
    dot_general x1, matrix products, expert_products(): lax.dot_general(expert_rows, d_gate, ROWS, preferred_element_type=F32)  3.32 us

profile of v1, /device:TPU:15, one launch (start us, length us, event | category | flops | bytes accessed | tf_op | source)
XLA Modules:
  0.0 139.7 jit_solution(12189077925793079933)
XLA Ops:
  0.6 0.0 copy-start
  0.6 0.9 copy.19.routes_ref
  1.6 0.8 copy.20.weight_ref
  2.4 1.0 copy-done.2
  3.4 1.0 copy-done.4
  4.4 0.9 copy-done.5
  5.3 0.7 copy-done.10
  6.0 51.2 %dispatch.1 = (bf16[2,16,64,2048]{3,2,1,0:T(8,128)(2,1)S(1)}, bf16[16,128,512]{2,1,0:T(8,128)(2,1)S(1)}, bf16[128,256]{1,0:T(8,128)(2,1)S(1)}, f32[128,128]{1,0:T(8,128)S(1)}) custom-call(bf16[128,2048]{1,0:T(8,128)(2,1)S(1)} %copy-done.4, bf16[128,2048]{1,0:T(8,128)(2,1)S(1)} %copy-done.2, s32[128,2]{1,0:T(8,128)S(1)} %copy.19.routes_ref, ...), custom_call_target="tpu_custom_call" | custom-call | tf_op jit(solution)/shard_map/dispatch/pallas_call | solution.py:604
  57.2 1.1 fusion.14
  58.3 2.2 %fusion.5 = f32[1024,448]{0,1:T(8,128)S(1)} fusion(bf16[1024,2048]{1,0:T(8,128)(2,1)S(1)} %bitcast.38, bf16[1,2048,448]{1,2,0:T(8,128)(2,1)S(1)} %copy-done), kind=kOutput, calls=%fused_computation.9 | convolution fusion | flops 1879048192 | bytes 7864320 | tf_op jit(solution)/shard_map/dot_general | solution.py:683
  60.5 2.1 %fusion.8 = f32[1024,448]{0,1:T(8,128)S(1)} fusion(bf16[1024,2048]{1,0:T(8,128)(2,1)S(1)} %bitcast.39, bf16[1,2048,448]{1,2,0:T(8,128)(2,1)S(1)} %copy-done.13), kind=kOutput, calls=%fused_computation.12 | convolution fusion | flops 1879048192 | bytes 7864320 | tf_op jit(solution)/shard_map/dot_general | solution.py:684
  62.6 0.0 copy-start.12
  62.6 3.4 %fusion = bf16[1,448,2048]{2,1,0:T(8,128)(2,1)} fusion(bf16[1024,2048]{1,0:T(8,128)(2,1)S(1)} %bitcast.42, f32[1024,448]{0,1:T(8,128)S(1)} %fusion.8, f32[1024,448]{0,1:T(8,128)S(1)} %fusion.5), kind=kOutput, calls=%fused_computation.4 | convolution fusion | flops 1882718208 | bytes 9699328 | tf_op jit(solution)/shard_map/dot_general | solution.py:688
  66.0 2.6 %multiply_convert_fusion.1 = (bf16[1024,448]{0,1:T(8,128)(2,1)S(1)}, bf16[1024,448]{0,1:T(8,128)(2,1)S(1)}) fusion(f32[1024,448]{0,1:T(8,128)S(1)} %fusion.5, f32[1024,448]{0,1:T(8,128)S(1)} %fusion.8, bf16[1024,2048]{1,0:T(8,128)(2,1)S(1)} %bitcast.43, bf16[1,448,2048]{2,1,0:T(8,128)(2,1)S(1)} %copy-done.12), kind=kOutput, calls=%fused_computation.17 | convolution fusion | flops 1885011968 | bytes 11534336 | tf_op jit(solution)/shard_map/dot_general | solution.py:687
  68.6 3.3 %fusion.2 = bf16[1,2048,448]{1,2,0:T(8,128)(2,1)} fusion(bf16[1024,448]{0,1:T(8,128)(2,1)S(1)} %get-tuple-element.22, bf16[1024,2048]{1,0:T(8,128)(2,1)S(1)} %bitcast.40), kind=kOutput, calls=%fused_computation.6 | convolution fusion | flops 1879965696 | bytes 6946816 | tf_op jit(solution)/shard_map/dot_general | solution.py:692
  72.0 3.3 %fusion.1 = bf16[1,2048,448]{1,2,0:T(8,128)(2,1)} fusion(bf16[1024,448]{0,1:T(8,128)(2,1)S(1)} %get-tuple-element.23, bf16[1024,2048]{1,0:T(8,128)(2,1)S(1)} %bitcast.41), kind=kOutput, calls=%fused_computation.5 | convolution fusion | flops 1879965696 | bytes 6946816 | tf_op jit(solution)/shard_map/dot_general | solution.py:691
  75.3 2.7 %fusion.3 = f32[1024,2048]{1,0:T(8,128)S(1)} fusion(bf16[1024,448]{0,1:T(8,128)(2,1)S(1)} %get-tuple-element.23, bf16[1,2048,448]{1,2,0:T(8,128)(2,1)S(1)} %copy-done), kind=kOutput, calls=%fused_computation.7 | convolution fusion | flops 1879048192 | bytes 11141120 | tf_op jit(solution)/shard_map/dot_general | solution.py:694
  78.0 0.0 copy-start.6
  78.0 0.0 copy-start.7
  78.0 4.6 %add_convert_fusion = bf16[1024,2048]{1,0:T(8,128)(2,1)} fusion(f32[1024,2048]{1,0:T(8,128)S(1)} %fusion.3, bf16[1024,448]{0,1:T(8,128)(2,1)S(1)} %get-tuple-element.22, bf16[1,2048,448]{1,2,0:T(8,128)(2,1)S(1)} %copy-done.13), kind=kOutput, calls=%fused_computation | convolution fusion | flops 1883242496 | bytes 15335424 | tf_op jit(solution)/shard_map/dot_general | solution.py:695
  82.6 55.1 %combine.1 = (f32[128,512]{1,0:T(8,128)S(1)}, bf16[128,512]{1,0:T(8,128)(2,1)S(1)}, bf16[128,512]{1,0:T(8,128)(2,1)S(1)}) custom-call(bf16[16,64,2048]{2,1,0:T(8,128)(2,1)} %bitcast.37, bf16[128,256]{1,0:T(8,128)(2,1)S(1)} %get-tuple-element.14.pt_ref, f32[128,128]{1,0:T(8,128)S(1)} %get-tuple-element.15.stat_ref, bf16[128,2048]{1,0:T(8,128)(2,1)S(1)} %copy-done.3, ...), custom_call_target="tpu_custom_call" | custom-call | tf_op jit(solution)/shard_map/combine/pallas_call | solution.py:640
  137.7 0.7 copy.24
  138.4 0.7 copy.25
  139.1 0.7 copy.26
  (20 shorter events, 0.1 us)
Async XLA Ops:
  0.6 57.7 %copy-start = (bf16[1,2048,448]{1,2,0:T(8,128)(2,1)S(1)}, bf16[1,2048,448]{1,2,0:T(8,128)(2,1)}, u32[]{:S(2)}) copy-start(bf16[1,2048,448]{1,2,0:T(8,128)(2,1)} %param.17) | copy-start | bytes 5505028
  2.4 1.0 copy-start.2
  3.4 1.0 copy-start.4
  4.4 0.9 copy-start.5
  5.3 0.7 copy-start.10
  58.3 2.2 %copy-start.13 = (bf16[1,2048,448]{1,2,0:T(8,128)(2,1)S(1)}, bf16[1,2048,448]{1,2,0:T(8,128)(2,1)}, u32[]{:S(2)}) copy-start(bf16[1,2048,448]{1,2,0:T(8,128)(2,1)} %param.18) | copy-start | bytes 5505028
  62.6 3.4 %copy-start.12 = (bf16[1,448,2048]{2,1,0:T(8,128)(2,1)S(1)}, bf16[1,448,2048]{2,1,0:T(8,128)(2,1)}, u32[]{:S(2)}) copy-start(bf16[1,448,2048]{2,1,0:T(8,128)(2,1)} %param.19) | copy-start | bytes 5505028
  78.0 4.6 %copy-start.1 = (bf16[2048,512]{1,0:T(8,128)(2,1)S(1)}, bf16[2048,512]{1,0:T(8,128)(2,1)}, u32[]{:S(2)}) copy-start(bf16[2048,512]{1,0:T(8,128)(2,1)} %proj_ref.1) | copy-start | bytes 6291460
  78.0 4.6 %copy-start.3 = (bf16[128,2048]{1,0:T(8,128)(2,1)S(1)}, bf16[128,2048]{1,0:T(8,128)(2,1)}, u32[]{:S(2)}) copy-start(bf16[128,2048]{1,0:T(8,128)(2,1)} %g_ref.3) | copy-start | bytes 1572868
  78.0 4.6 %copy-start.6 = (bf16[128,512]{1,0:T(8,128)(2,1)S(1)}, bf16[128,512]{1,0:T(8,128)(2,1)}, u32[]{:S(2)}) copy-start(bf16[128,512]{1,0:T(8,128)(2,1)} %conv_ref.3) | copy-start | bytes 393220
  78.0 4.6 %copy-start.7 = (bf16[128,512]{1,0:T(8,128)(2,1)S(1)}, bf16[128,512]{1,0:T(8,128)(2,1)}, u32[]{:S(2)}) copy-start(bf16[128,512]{1,0:T(8,128)(2,1)} %value_ref.1) | copy-start | bytes 393220
  78.0 4.6 %copy-start.8 = (bf16[128,512]{1,0:T(8,128)(2,1)S(1)}, bf16[128,512]{1,0:T(8,128)(2,1)}, u32[]{:S(2)}) copy-start(bf16[128,512]{1,0:T(8,128)(2,1)} %gate_ref.1) | copy-start | bytes 393220
  78.0 4.6 %copy-start.9 = (f32[31,512]{1,0:T(8,128)S(1)}, f32[31,512]{1,0:T(8,128)}, u32[]{:S(2)}) copy-start(f32[31,512]{1,0:T(8,128)} %taps_ref.1) | copy-start | bytes 190468
  78.0 4.6 %copy-start.11 = (f32[512]{0:T(512)S(1)}, f32[512]{0:T(512)}, u32[]{:S(2)}) copy-start(f32[512]{0:T(512)} %param.25) | copy-start | bytes 6148

commit v2 on v1

--- a/solution.py
+++ b/solution.py
@@ -244,14 +244,13 @@
 
 
 def dispatch_kernel(
-    groups, x_ref, g_ref, routes_ref, weight_ref, conv_ref, gain_ref,
-    xo, mo, pt_ref, stat_ref,
-    sb, xs, ms, st, st_in,
+    groups, x_hbm, g_hbm, routes_ref, weight_ref, conv_hbm, gain_ref, gw_hbm, uw_hbm, dw_hbm,
+    xo, co, mo, pt_ref, stat_ref, hid_ref, dg_ref, du_ref,
+    x_ref, g_ref, conv_ref, gw, uw, dw, sb, xs, ms, st, st_in,
     z_s, z_r, x_s, x_r, y_s, y_r, a_s, a_r, b_s, b_r, c_s, c_r,
-    mz_s, mz_r, mx_s, mx_r, mc_s, mc_r, st_s, st_r, o_s, mo_s,
+    mz_s, mz_r, mx_s, mx_r, mc_s, mc_r, st_s, st_r, o_s, mo_s, w_s,
 ):
     s, t, u, q, r, _, _, rx, rc, rxc = place()
-    n_sp = groups * SPAN
     tok, width = x_ref.shape
     cap = sb.shape[2]
     half = width // 2
@@ -262,8 +261,23 @@
     peers = [(lax.rem(q + d, groups) * SPAN + r, t) for d in order[1:]]
     ready = greet(peers + [at_x, at_c, at_y])
 
+    pairs = [(x_hbm, x_ref), (g_hbm, g_ref), (conv_hbm, conv_ref), (gw_hbm, gw), (uw_hbm, uw), (dw_hbm, dw)]
+    loads = [
+        pltpu.make_async_copy(src, dst, w_s.at[i])
+        for i, (src, dst) in enumerate(pairs)
+    ]
+    for copy in loads:
+        copy.start()
+
     lane = lax.broadcasted_iota(jnp.int32, (tok, 128), 1)
-    hot = [(routes_ref[:, k : k + 1] == lane).astype(F32) for k in range(2)]
+    eye = lane == lax.broadcasted_iota(jnp.int32, (tok, tok), 0)
+
+    def column(row):
+        return jnp.sum(jnp.where(eye, row, jnp.zeros_like(row)), axis=1, keepdims=True)
+
+    routes = [column(routes_ref[k : k + 1, :].astype(F32)).astype(jnp.int32) for k in range(2)]
+    weights = [column(weight_ref[k : k + 1, :]) for k in range(2)]
+    hot = [(routes[k] == lane).astype(F32) for k in range(2)]
     before = (
         lax.broadcasted_iota(jnp.int32, (tok, tok), 1) < lax.broadcasted_iota(jnp.int32, (tok, tok), 0)
     ).astype(BF16)
@@ -272,11 +286,13 @@
     pts, cots = [], []
     for k in range(2):
         slot = jnp.sum(counts * hot[k], axis=1, keepdims=True).astype(jnp.int32)
-        target = routes_ref[:, k : k + 1] * cap + slot
+        target = routes[k] * cap + slot
         pts.append((target == spots).astype(F32).astype(BF16))
     pt = pts[0] + pts[1]
     pt_ref[...] = pt
     chunk = 512
+    for copy in loads[:3]:
+        copy.wait()
     for j in range(0, width, chunk):
         cols = slice(j, j + chunk)
         rows = lax.dot_general(pt, x_ref[:, cols], ROWS, preferred_element_type=F32)
@@ -286,7 +302,7 @@
         for k in range(2):
             part = lax.dot_general(
                 pts[k],
-                (weight_ref[:, k : k + 1] * cot).astype(BF16),
+                (weights[k] * cot).astype(BF16),
                 ROWS,
                 preferred_element_type=F32,
             )
@@ -298,7 +314,7 @@
     st[...] = jnp.where(lane == 0, first, second)
     ready()
 
-    started = []
+    started, outs = [], []
 
     def go(copy):
         copy.start()
@@ -352,9 +368,24 @@
             got = xs.at[:, base + place_in, :, cols]
             send(got, got, c_s.at[d, i], c_r.at[d, i], *at_c).wait_recv()
         span = pl.ds(base, SPAN)
-        out = pltpu.make_async_copy(xs.at[:, span], xo.at[:, span], o_s.at[d])
-        out.start()
-        return out
+        for i, dst in enumerate([xo, co]):
+            out = pltpu.make_async_copy(xs.at[i, span], dst.at[span], o_s.at[d, i])
+            out.start()
+            outs.append(out)
+        if d == 0:
+            for copy in loads[3:]:
+                copy.wait()
+        rows = xs[0, span].reshape(SPAN * cap, width)
+        cot = xs[1, span].reshape(SPAN * cap, width)
+        gate_pre = lax.dot_general(rows, gw[...], UNITS, preferred_element_type=F32)
+        up_pre = lax.dot_general(rows, uw[...], UNITS, preferred_element_type=F32)
+        d_hidden = lax.dot_general(cot, dw[...], UNITS, preferred_element_type=F32)
+        sig = jax.nn.sigmoid(gate_pre)
+        silu = gate_pre * sig
+        into = pl.ds(pl.multiple_of(base * cap, SPAN * cap), SPAN * cap)
+        hid_ref[into, :] = (silu * up_pre).astype(BF16)
+        dg_ref[into, :] = (d_hidden * up_pre * swish_slope(gate_pre, sig)).astype(BF16)
+        du_ref[into, :] = (d_hidden * silu).astype(BF16)
 
     stage_one(0)
     xs[:, s, :, mine] = sb[:, q, :, mine]
@@ -370,7 +401,6 @@
         to = lax.rem(q + d, groups)
         go(send(ms.at[s], ms.at[s], mz_s.at[d], mz_r.at[d], to * SPAN + r, t))
 
-    outs = []
     for i in range(groups + 2):
         if 0 < i < groups:
             stage_one(order[i])
@@ -384,12 +414,13 @@
                 send(got, got, mz_s.at[d], mz_r.at[d], s, t).wait_recv()
             go(send(got, got, mx_s.at[d], mx_r.at[d], *at_x))
             go(send(got, got, mc_s.at[d, 0], mc_r.at[d, 0], *at_c))
-    for d in order:
-        outs.append(finish(d))
+        if i > 2:
+            finish(order[i - 3])
     for d in order:
         got = ms.at[lax.rem(q - d + groups, groups) * SPAN + rx]
         send(got, got, mx_s.at[d], mx_r.at[d], *at_x).wait_recv()
         go(send(got, got, mc_s.at[d, 1], mc_r.at[d, 1], *at_c))
+    finish(order[-1])
     for d in order:
         base = lax.rem(q - d + groups, groups) * SPAN
         for i, place_in in enumerate([rc, rxc]):
@@ -405,9 +436,9 @@
 
 
 def combine_kernel(
-    groups, t_ref, pt_ref, stat_ref, g_ref, proj_ref, conv_ref, gain_ref, value_ref, gate_ref, taps_ref, m_ref,
+    groups, dg_ref, du_ref, gw_ref, uw_ref, pt_ref, stat_ref, g_ref, proj_ref, conv_ref, gain_ref, value_ref, gate_ref, taps_ref, m_ref,
     gp_ref, gv_ref, gg_ref,
-    core_in, s1, rx1, ry1, sa, sbb, rx2, ry2, fin, rz, rt, rr, st, st_in, ext, halo, halo_in, slope_ref, normed_ref,
+    t_ref, core_in, s1, rx1, ry1, sa, sbb, rx2, ry2, fin, rz, rt, rr, st, st_in, ext, halo, halo_in, slope_ref, normed_ref,
     c_s, c_r, x1_s, x1_r, y1_s, y1_r, x2_s, x2_r, y2_s, y2_r, z_s, z_r,
     h_s, h_r, k_s, k_r, st_s, st_r, halo_s, halo_r,
 ):
@@ -436,8 +467,16 @@
         return (a.astype(F32) + b.astype(F32)).astype(BF16)
 
     ready()
-    for d in order:
+
+    def products(d):
         to = lax.rem(q + d, groups)
+        rows = pl.ds(pl.multiple_of(to * (SPAN * cap), SPAN * cap), SPAN * cap)
+        chunk = 512
+        for j in range(0, width, chunk):
+            cols = slice(j, j + chunk)
+            part = jnp.dot(dg_ref[rows, :], gw_ref[:, cols], preferred_element_type=F32)
+            part = part + jnp.dot(du_ref[rows, :], uw_ref[:, cols], preferred_element_type=F32)
+            t_ref[pl.ds(to * SPAN, SPAN), :, cols] = part.astype(BF16).reshape(SPAN, cap, chunk)
         for i in range(2):
             go(send(t_ref.at[to * SPAN + 2 * i + cb], core_in.at[d, i], c_s.at[d, i], c_r.at[d, i], *at_c))
 
@@ -476,7 +515,10 @@
             rz[q, :, :piece] = low
             rz[q, :, piece:] = high
 
+    products(order[0])
     for i in range(groups + 2):
+        if i + 1 < groups:
+            products(order[i + 1])
         if i < groups:
             stage_one(order[i])
         if i == 1:
@@ -599,19 +641,34 @@
     cap = SPAN * min(tok // SPAN, 2 * tok // (groups * SPAN))
     vmem = pl.BlockSpec(memory_space=pltpu.VMEM)
     hbm = pl.BlockSpec(memory_space=pl.ANY)
+    pinned = pl.BlockSpec(memory_space=pltpu.MemorySpace.HBM)
     dma = pltpu.SemaphoreType.DMA
     gain = norm_gain[None]
-    rows, mixed_all, pt, stat = pl.pallas_call(
+    gate_w, up_w = jnp.swapaxes(w_gate[0], 0, 1), jnp.swapaxes(w_up[0], 0, 1)
+    down_w = w_down[0]
+    units = down_w.shape[0]
+    unit_rows = jax.ShapeDtypeStruct((n_sp * cap, units), BF16)
+    expert_rows, expert_cot, mixed_all, pt, stat, hidden, d_gate, d_up = pl.pallas_call(
         functools.partial(dispatch_kernel, groups),
         out_shape=(
-            jax.ShapeDtypeStruct((2, n_sp, cap, width), BF16),
+            jax.ShapeDtypeStruct((n_sp, cap, width), BF16),
+            jax.ShapeDtypeStruct((n_sp, cap, width), BF16),
             jax.ShapeDtypeStruct((n_sp, tok, channels), BF16),
             jax.ShapeDtypeStruct((tok, groups * cap), BF16),
             jax.ShapeDtypeStruct((tok, 128), F32),
+            unit_rows,
+            unit_rows,
+            unit_rows,
         ),
-        in_specs=[vmem] * 6,
-        out_specs=(hbm, hbm, vmem, vmem),
+        in_specs=[pinned, pinned, vmem, vmem, pinned, vmem] + [pinned] * 3,
+        out_specs=(hbm,) * 3 + (vmem,) * 5,
         scratch_shapes=[
+            pltpu.VMEM((tok, width), BF16),
+            pltpu.VMEM((tok, width), BF16),
+            pltpu.VMEM((tok, channels), BF16),
+        ]
+        + [pltpu.VMEM((units, width), BF16)] * 3
+        + [
             pltpu.VMEM((2, groups, cap, width), BF16),
             pltpu.VMEM((2, n_sp, cap, width), BF16),
             pltpu.VMEM((n_sp, tok, channels), BF16),
@@ -623,15 +680,20 @@
         + [dma((groups,))] * 4
         + [dma((groups, 2))] * 2
         + [dma] * 2
-        + [dma((groups,)), dma],
+        + [dma((groups, 2)), dma, dma((6,))],
         compiler_params=pltpu.CompilerParams(
-            collective_id=0, has_side_effects=True, vmem_limit_bytes=36 << 20
+            collective_id=0, has_side_effects=True, vmem_limit_bytes=63 << 20
         ),
         name="dispatch",
-    )(moe_input, out_cotangent, routes, route_weight, conv_out, gain)
-    expert_rows = rows[0].reshape(n_sp * cap, width)
-    expert_cot = rows[1].reshape(n_sp * cap, width)
-    grad_gate, grad_up, grad_down, part = expert_products(expert_rows, expert_cot, w_gate, w_up, w_down)
+    )(moe_input, out_cotangent, routes.T, route_weight.T, conv_out, gain, gate_w, up_w, down_w)
+    expert_rows = expert_rows.reshape(n_sp * cap, width)
+    expert_cot = expert_cot.reshape(n_sp * cap, width)
+    grad_down = lax.dot_general(hidden, expert_cot, ROWS, preferred_element_type=F32).astype(BF16)
+    grad_gate = lax.dot_general(expert_rows, d_gate, ROWS, preferred_element_type=F32).astype(BF16)
+    grad_up = lax.dot_general(expert_rows, d_up, ROWS, preferred_element_type=F32).astype(BF16)
+    grad_gate, grad_up, grad_down, d_gate, d_up = lax.optimization_barrier(
+        (grad_gate, grad_up, grad_down, d_gate, d_up)
+    )
     reach = -(-(WIDTH - 1) // 16) * 16
     half = width // 2
     piece = half // 2
@@ -644,9 +706,10 @@
             jax.ShapeDtypeStruct((tok, channels), BF16),
             jax.ShapeDtypeStruct((tok, channels), BF16),
         ),
-        in_specs=[vmem] * 11,
+        in_specs=[vmem] * 14,
         out_specs=(vmem,) * 3,
         scratch_shapes=[
+            pltpu.VMEM((n_sp, cap, width), BF16),
             pltpu.VMEM((groups, 2, cap, width), BF16),
             pltpu.VMEM((groups, 2, 2, 2, cap, piece), BF16),
             pair, pair, pair, pair, single, single,
@@ -672,29 +735,10 @@
         ),
         name="combine",
     )(
-        part.reshape(n_sp, cap, width),
+        d_gate, d_up, gate_w, up_w,
         pt, stat, out_cotangent, out_proj, conv_out, gain, glu_value, glu_gate, taps, mixed_all,
     )
-    return (grad_gate, grad_up, grad_down, grad_proj, grad_value, grad_gate_in)
-
-
-def expert_products(expert_rows, expert_cot, w_gate, w_up, w_down):
-    gate_w, up_w, down_w = w_gate[0], w_up[0], w_down[0]
-    gate_pre = jnp.dot(expert_rows, gate_w, preferred_element_type=F32)
-    up_pre = jnp.dot(expert_rows, up_w, preferred_element_type=F32)
-    gate_sig = jax.nn.sigmoid(gate_pre)
-    hidden = (gate_pre * gate_sig * up_pre).astype(BF16)
-    d_hidden = lax.dot_general(expert_cot, down_w, UNITS, preferred_element_type=F32)
-    grad_down = lax.dot_general(hidden, expert_cot, ROWS, preferred_element_type=F32).astype(BF16)
-    d_gate = (d_hidden * up_pre * swish_slope(gate_pre, gate_sig)).astype(BF16)
-    d_up = (d_hidden * gate_pre * gate_sig).astype(BF16)
-    grad_gate = lax.dot_general(expert_rows, d_gate, ROWS, preferred_element_type=F32).astype(BF16)
-    grad_up = lax.dot_general(expert_rows, d_up, ROWS, preferred_element_type=F32).astype(BF16)
-    part = (
-        lax.dot_general(d_gate, gate_w, UNITS, preferred_element_type=F32)
-        + lax.dot_general(d_up, up_w, UNITS, preferred_element_type=F32)
-    ).astype(BF16)
-    return grad_gate[None], grad_up[None], grad_down[None], part
+    return (grad_gate[None], grad_up[None], grad_down[None], grad_proj, grad_value, grad_gate_in)
 
 
 def solution(mesh):

time: 140 us -> 129 us (0.921)
  matrix products: 24.1 us -> 13 us
  Pallas kernels: 106 us -> 113 us
  local copies, waits for them, and re-layouts: 8.53 us -> 2.08 us
    dot_general x8 -> x3, matrix products: 24.1 us -> 13 us  [the longest x1 5.98 us: paired(): lax.dot_general(expert_rows, d_up, ROWS, preferred_element_type=F32)]
    unnamed x33 -> x31, local copies, waits for them, and re-layouts: 7.45 us -> 2.08 us
    pallas_call x1, Pallas kernels: 51.2 us -> 55.4 us  [paired(): pl.pallas_call(functools.partial(dispatch_kernel, groups), out_shape=(jax...]
    pallas_call x1, Pallas kernels: 55.1 us -> 57.4 us  [paired(): pl.pallas_call(functools.partial(combine_kernel, groups), out_shape=(jax....]
where the time goes in v2:
time: 129 us
  Pallas kernels  113 us (88%)
  matrix products  13 us (10%)
  local copies, waits for them, and re-layouts  2.08 us (2%)
    pallas_call x1, Pallas kernels, paired(): pl.pallas_call(functools.partial(combine_kernel, groups), out_shape=(jax....  57.4 us
    pallas_call x1, Pallas kernels, paired(): pl.pallas_call(functools.partial(dispatch_kernel, groups), out_shape=(jax...  55.4 us
    dot_general x1, matrix products, paired(): lax.dot_general(expert_rows, d_up, ROWS, preferred_element_type=F32)  5.98 us
    dot_general x1, matrix products, paired(): lax.dot_general(hidden, expert_cot, ROWS, preferred_element_type=F32)  3.58 us
    dot_general x1, matrix products, paired(): lax.dot_general(expert_rows, d_gate, ROWS, preferred_element_type=F32)  3.42 us

profile of v2, /device:TPU:15, one launch (start us, length us, event | category | flops | bytes accessed | tf_op | source)
XLA Modules:
  0.0 128.6 jit_solution(5490849845874876870)
XLA Ops:
  0.6 55.4 %dispatch.1 = (bf16[16,64,2048]{2,1,0:T(8,128)(2,1)}, bf16[16,64,2048]{2,1,0:T(8,128)(2,1)}, bf16[16,128,512]{2,1,0:T(8,128)(2,1)}, bf16[128,256]{1,0:T(8,128)(2...) custom-call(bf16[128,2048]{1,0:T(8,128)(2,1)} %x_hbm.1, ...), custom_call_target="tpu_custom_call" | custom-call | tf_op jit(solution)/shard_map/dispatch/pallas_call | solution.py:651
  56.0 0.0 copy-start.2
  56.0 0.0 copy-start.12
  56.0 6.0 %convolution_convert_fusion.1 = bf16[2048,448]{0,1:T(8,128)(2,1)} fusion(bf16[1024,2048]{1,0:T(8,128)(2,1)} %bitcast.31, bf16[1024,448]{1,0:T(8,128)(2,1)} %get-tuple-element.31.du_ref), kind=kOutput, calls=%fused_computation.1 | convolution fusion | flops 1879965696 | bytes 6946816 | tf_op jit(solution)/shard_map/dot_general | solution.py:693
  62.0 0.0 copy-done.2
  62.0 0.0 copy-done.12
  62.0 0.0 copy-start.13
  62.0 3.4 %convolution_convert_fusion.2 = bf16[2048,448]{0,1:T(8,128)(2,1)} fusion(bf16[1024,2048]{1,0:T(8,128)(2,1)S(1)} %bitcast.32, bf16[1024,448]{1,0:T(8,128)(2,1)S(1)} %copy-done.2), kind=kOutput, calls=%fused_computation.2 | convolution fusion | flops 1879965696 | bytes 6946816 | tf_op jit(solution)/shard_map/dot_general | solution.py:692
  65.5 0.0 copy-done.11
  65.5 0.0 copy-done.13
  65.5 0.0 copy-start.3
  65.5 0.0 copy-start.4
  65.5 0.0 copy-start.5
  65.5 0.0 copy-start.6
  65.5 0.0 copy-start.7
  65.5 0.0 copy-start.8
  65.5 0.0 copy-start.9
  65.5 0.0 copy-start.10
  65.6 3.6 %convolution_convert_fusion = bf16[448,2048]{1,0:T(8,128)(2,1)} fusion(bf16[1024,448]{1,0:T(8,128)(2,1)S(1)} %copy-done.13, bf16[1024,2048]{1,0:T(8,128)(2,1)S(1)} %bitcast.30), kind=kOutput, calls=%fused_computation | convolution fusion | flops 1879965696 | bytes 6946816 | tf_op jit(solution)/shard_map/dot_general | solution.py:691
  69.1 0.0 copy-done.1
  69.2 57.4 %combine.1 = (f32[128,512]{1,0:T(8,128)S(1)}, bf16[128,512]{1,0:T(8,128)(2,1)S(1)}, bf16[128,512]{1,0:T(8,128)(2,1)S(1)}) custom-call(bf16[1024,448]{1,0:T(8,128)(2,1)S(1)} %copy-done.2, bf16[1024,448]{1,0:T(8,128)(2,1)S(1)} %copy-done.3, bf16[448,2048]{1,0:T(8,128)(2,1)S(1)} %bitcast.22, bf16[448,2048]{1,0:T(8,128)(2,1)} %bitcast.26, ...), custom_call_target="tpu_custom_call" | custom-call | tf_op jit(solution)/shard_map/combine/pallas_call | solution.py:702
  126.6 0.7 copy.22
  127.3 0.7 copy.23
  128.0 0.7 copy.24
  (12 shorter events, 0.0 us)
Async XLA Ops:
  56.0 6.0 %copy-start.2 = (bf16[1024,448]{1,0:T(8,128)(2,1)S(1)}, bf16[1024,448]{1,0:T(8,128)(2,1)}, u32[]{:S(2)}) copy-start(bf16[1024,448]{1,0:T(8,128)(2,1)} %get-tuple-element.30.dg_ref) | copy-start | bytes 2752516
  56.0 6.0 %copy-start.12 = (bf16[16,64,2048]{2,1,0:T(8,128)(2,1)S(1)}, bf16[16,64,2048]{2,1,0:T(8,128)(2,1)}, u32[]{:S(2)}) copy-start(bf16[16,64,2048]{2,1,0:T(8,128)(2,1)} %get-tuple-element.22) | copy-start | bytes 12582916
  62.0 3.4 %copy-start.11 = (bf16[16,64,2048]{2,1,0:T(8,128)(2,1)S(1)}, bf16[16,64,2048]{2,1,0:T(8,128)(2,1)}, u32[]{:S(2)}) copy-start(bf16[16,64,2048]{2,1,0:T(8,128)(2,1)} %get-tuple-element.26) | copy-start | bytes 12582916
  62.0 3.4 %copy-start.13 = (bf16[1024,448]{1,0:T(8,128)(2,1)S(1)}, bf16[1024,448]{1,0:T(8,128)(2,1)}, u32[]{:S(2)}) copy-start(bf16[1024,448]{1,0:T(8,128)(2,1)} %get-tuple-element.25) | copy-start | bytes 2752516
  65.5 3.7 %copy-start = (bf16[1,2048,448]{1,2,0:T(8,128)(2,1)S(1)}, bf16[1,2048,448]{1,2,0:T(8,128)(2,1)}, u32[]{:S(2)}) copy-start(bf16[1,2048,448]{1,2,0:T(8,128)(2,1)} %param.17) | copy-start | bytes 5505028
  65.5 3.7 %copy-start.1 = (bf16[128,2048]{1,0:T(8,128)(2,1)S(1)}, bf16[128,2048]{1,0:T(8,128)(2,1)}, u32[]{:S(2)}) copy-start(bf16[128,2048]{1,0:T(8,128)(2,1)} %g_ref.1) | copy-start | bytes 1572868
  65.5 3.7 %copy-start.3 = (bf16[1024,448]{1,0:T(8,128)(2,1)S(1)}, bf16[1024,448]{1,0:T(8,128)(2,1)}, u32[]{:S(2)}) copy-start(bf16[1024,448]{1,0:T(8,128)(2,1)} %get-tuple-element.31.du_ref) | copy-start | bytes 2752516
  65.5 3.7 %copy-start.4 = (bf16[128,512]{1,0:T(8,128)(2,1)S(1)}, bf16[128,512]{1,0:T(8,128)(2,1)}, u32[]{:S(2)}) copy-start(bf16[128,512]{1,0:T(8,128)(2,1)} %conv_ref.1) | copy-start | bytes 393220
  65.5 3.7 %copy-start.5 = (bf16[128,512]{1,0:T(8,128)(2,1)S(1)}, bf16[128,512]{1,0:T(8,128)(2,1)}, u32[]{:S(2)}) copy-start(bf16[128,512]{1,0:T(8,128)(2,1)} %value_ref.1) | copy-start | bytes 393220
  65.5 3.7 %copy-start.6 = (bf16[128,512]{1,0:T(8,128)(2,1)S(1)}, bf16[128,512]{1,0:T(8,128)(2,1)}, u32[]{:S(2)}) copy-start(bf16[128,512]{1,0:T(8,128)(2,1)} %gate_ref.1) | copy-start | bytes 393220
  65.5 3.7 %copy-start.7 = (f32[31,512]{1,0:T(8,128)S(1)}, f32[31,512]{1,0:T(8,128)}, u32[]{:S(2)}) copy-start(f32[31,512]{1,0:T(8,128)} %taps_ref.1) | copy-start | bytes 190468
  65.5 3.7 %copy-start.8 = (bf16[128,256]{1,0:T(8,128)(2,1)S(1)}, bf16[128,256]{1,0:T(8,128)(2,1)}, u32[]{:S(2)}) copy-start(bf16[128,256]{1,0:T(8,128)(2,1)} %get-tuple-element.32.pt_ref) | copy-start | bytes 196612
  65.5 3.7 %copy-start.9 = (f32[128,128]{1,0:T(8,128)S(1)}, f32[128,128]{1,0:T(8,128)}, u32[]{:S(2)}) copy-start(f32[128,128]{1,0:T(8,128)} %get-tuple-element.33.stat_ref) | copy-start | bytes 196612
  65.5 3.7 %copy-start.10 = (f32[512]{0:T(512)S(1)}, f32[512]{0:T(512)}, u32[]{:S(2)}) copy-start(f32[512]{0:T(512)} %param.25) | copy-start | bytes 6148
